TPU v7x, 128 devices: a whole 4x4x4 slice. The times are simulated.
128 devices in a mesh: sp: 16 (over z, x), tp: 8 (over y, core).
Axes of the slice: x: 4, y: 4, z: 4, core: 2. Of those that a mesh axis runs over, the one named last changes fastest.
Arguments:
- queries: bfloat16 [16384, 1024], P('sp', 'tp'), may hold values from -6 to 6, as said below
- key_rows: bfloat16 [16384, 1024], P('sp', 'tp'), may hold values from -6 to 6, as said below
- value_rows: bfloat16 [16384, 1024], P('sp', 'tp'), may hold values from -6 to 6
- lambdas: float32 [8], P('tp'), may hold values from 0.3 to 0.8
- head_gain: float32 [128], replicated, may hold values from 0.1 to 1.9
- out_weight: bfloat16 [1024, 2048], replicated, may hold values from -0.1875 to 0.1875
- stream: bfloat16 [16384, 2048], P(('sp', 'tp')), may hold values from -6 to 6
- ffn_gain: float32 [2048], replicated, may hold values from 0.1 to 1.9
- routes: int32 [16384, 2], P(('sp', 'tp')), may hold values from 0 to 15, all different within a row; in each aligned block of 128 rows (0 to 127, 128 to 255, ...) at most 20 rows name the same one
- route_weight: float32 [16384, 2], P(('sp', 'tp')), may hold values from 0.1 to 1
- gate_weight: bfloat16 [16, 2048, 5120], P('sp', None, 'tp'), may hold values from -0.125 to 0.125
- up_weight: bfloat16 [16, 2048, 5120], P('sp', None, 'tp'), may hold values from -0.125 to 0.125
- down_weight: bfloat16 [16, 5120, 2048], P('sp', 'tp'), may hold values from -0.078125 to 0.078125
Outputs:
- layer_out: bfloat16 [16384, 2048], P(('sp', 'tp'))
Inputs may be any that keep to these rules, and one draw needn't show every extreme that they name: Custom draw; the queries of a position meet only keys of the same or earlier positions. `key_rows`: custom draw. `routes`: each row names 2 different experts. In the 128 rows of one device no expert is named by more than 20 rows, and every draw reaches 20 on some device.
All inputs are finite; a program needn't handle non-finite values.
Results may differ from a plain program's by a relative error of at most 0.01.
Values may be sent and summed in bfloat16 or wider, within the bound.
No kernel may reach another device: no remote copies, remote signals or barrier semaphores. Data moves between devices by JAX's collectives and lax.ppermute only.
A program may use at most 128 MiB of HBM per device.

v0:
```python
import math
import jax
import jax.numpy as jnp
from jax import lax
from jax.sharding import PartitionSpec as P

DH = 64


def side_by_side(arrays, axis, dim, along):
    both = jnp.concatenate(arrays, axis=along)
    filled, at, gathered = (lax.all_gather(both, axis, axis=dim, tiled=True), 0, [])
    for a in arrays:
        gathered.append(lax.slice_in_dim(filled, at, at + a.shape[along], axis=along))
        at += a.shape[along]
    return tuple(gathered)


def expert_rows(rows_in, gate_local, up_local, down_local):
    flat = rows_in.reshape(-1, rows_in.shape[-1])
    gate = jnp.dot(flat, gate_local, preferred_element_type=jnp.float32)
    upper = jnp.dot(flat, up_local, preferred_element_type=jnp.float32)
    act = (jax.nn.silu(gate) * upper).astype(jnp.bfloat16)
    result = jnp.dot(act, down_local, preferred_element_type=jnp.float32)
    return result.reshape(rows_in.shape)


def local(
    queries,
    key_rows,
    value_rows,
    lambdas,
    head_gain,
    out_weight,
    stream,
    ffn_gain,
    routes,
    route_weight,
    gate_weight,
    up_weight,
    down_weight,
):
    length = queries.shape[0]
    head_count = queries.shape[1] // (2 * DH)
    query_heads = queries.reshape(length, head_count, 2, DH)
    offset = lax.axis_index("sp") * length
    query_pos = offset + jnp.arange(length, dtype=jnp.int32)
    last_pos = offset + length - 1
    scale = DH ** (-0.5)
    initial = (
        jnp.full((head_count, 2, length), -1e30, jnp.float32),
        jnp.zeros((head_count, 2, length), jnp.float32),
        jnp.zeros((head_count, 2, length, 2 * DH), jnp.float32),
    )
    key_piece, value_piece = side_by_side((key_rows, value_rows), "sp", 0, 1)
    count = key_piece.shape[0]
    block = math.gcd(count, 512)

    def advance(number, state):
        begin = number * block
        key_block = lax.dynamic_slice_in_dim(key_piece, begin, block, 0).reshape(
            block, head_count, 2, DH
        )
        value_block = lax.dynamic_slice_in_dim(value_piece, begin, block, 0).reshape(
            block, head_count, 2 * DH
        )
        key_pos = begin + jnp.arange(block, dtype=jnp.int32)

        def compute(inner):
            maxima, totals, accum = inner
            scores = (
                jnp.einsum(
                    "qhmd,khmd->hmqk", query_heads, key_block, preferred_element_type=jnp.float32
                )
                * scale
            )
            mask = key_pos[None, :] <= query_pos[:, None]
            scores = jnp.where(mask, scores, -jnp.inf)
            fresh = jnp.maximum(maxima, jnp.max(scores, axis=-1))
            expo = jnp.exp(scores - fresh[..., None])
            factor = jnp.exp(maxima - fresh)
            totals = totals * factor + jnp.sum(expo, axis=-1)
            accum = accum * factor[..., None] + jnp.einsum(
                "hmqk,khe->hmqe",
                expo.astype(jnp.bfloat16),
                value_block,
                preferred_element_type=jnp.float32,
            )
            return (fresh, totals, accum)

        return lax.cond(begin <= last_pos, compute, lambda inner: inner, state)

    maxima, totals, accum = lax.fori_loop(0, count // block, advance, initial)
    mixed = accum / totals[..., None]
    contrast = mixed[:, 0] - lambdas[:, None, None] * mixed[:, 1]
    contrast = (
        contrast
        * lax.rsqrt(jnp.mean(contrast * contrast, axis=-1, keepdims=True) + 1e-05)
        * head_gain
    )
    heads_out = (
        jnp.transpose(contrast, (1, 0, 2)).reshape(length, head_count * 2 * DH).astype(jnp.bfloat16)
    )
    heads_local = lax.all_to_all(heads_out, "tp", split_axis=0, concat_axis=1, tiled=True)
    attended = stream.astype(jnp.float32) + jnp.dot(
        heads_local, out_weight, preferred_element_type=jnp.float32
    )
    normed = (
        attended
        * lax.rsqrt(jnp.mean(attended * attended, axis=-1, keepdims=True) + 1e-06)
        * ffn_gain
    ).astype(jnp.bfloat16)
    rows_local = normed.shape[0]
    width = normed.shape[1]
    top_count = routes.shape[1]
    sp_size = lax.axis_size("sp")
    experts = sp_size * gate_weight.shape[0]
    slots = max(2, (rows_local * top_count * 5 + 4 * experts - 1) // (4 * experts))
    flat_routes = routes.reshape(-1)
    onehot = (flat_routes[:, None] == jnp.arange(experts, dtype=jnp.int32)[None, :]).astype(
        jnp.int32
    )
    before = jnp.cumsum(onehot, axis=0) - onehot
    slot = jnp.sum(before * onehot, axis=1)
    target = flat_routes * slots + slot
    placed = (target[:, None] == jnp.arange(experts * slots, dtype=jnp.int32)[None, :]).astype(
        jnp.float32
    )
    placed = placed.reshape(rows_local, top_count, experts * slots)
    dispatch = jnp.transpose(jnp.sum(placed, axis=1)).astype(jnp.bfloat16)
    combine = jnp.einsum("tk,tks->ts", route_weight, placed)
    outgoing = (
        jnp.dot(dispatch, normed, preferred_element_type=jnp.float32)
        .astype(jnp.bfloat16)
        .reshape(experts, slots, width)
    )
    gate_local = gate_weight[0]
    up_local = up_weight[0]
    down_local = down_weight[0]
    arrived = lax.all_to_all(outgoing, "sp", split_axis=0, concat_axis=0, tiled=True)
    partial_value = expert_rows(
        lax.all_gather(arrived[:, None], "tp", axis=1, tiled=True), gate_local, up_local, down_local
    )
    summed = lax.psum_scatter(
        partial_value.astype(jnp.bfloat16), "tp", scatter_dimension=1, tiled=True
    )
    returned = lax.all_to_all(summed, "sp", split_axis=0, concat_axis=0, tiled=True).reshape(
        experts * slots, width
    )
    routed = jnp.dot(combine, returned.astype(jnp.float32))
    return (attended + routed).astype(jnp.bfloat16)


def solution(mesh):
    placed = (
        P("sp", "tp"),
        P("sp", "tp"),
        P("sp", "tp"),
        P("tp"),
        P(),
        P(),
        P(("sp", "tp"), None),
        P(),
        P(("sp", "tp"), None),
        P(("sp", "tp"), None),
        P("sp", None, "tp"),
        P("sp", None, "tp"),
        P("sp", "tp", None),
    )
    return jax.shard_map(
        local, mesh=mesh, in_specs=placed, out_specs=P(("sp", "tp"), None), check_vma=False
    )
```

profile of v0, /device:TPU:9, one launch (start us, length us, event | category | flops | bytes accessed | tf_op | source)
XLA Modules:
  0.0 605.6 jit_solution(11017342687480843919)
XLA Ops:
  6.5 2.0 pad_maximum_fusion
  11.5 1.1 copy.88
  12.6 70.0 %all-gather.4.cloned.1.call-done = bf16[16384,256]{1,0:T(8,128)(2,1)} async-done(((bf16[1024,256]{1,0:T(8,128)(2,1)}), bf16[16384,256]{1,0:T(8,128)(2,1)}) %all-gather.4.cloned.1.call-update) | async-done | bytes 8388624 | tf_op jit(solution)/shard_map/all_gather | solution.py:12
  82.6 5.7 fusion.36
  88.3 6.4 %copy.89 = bf16[16384,128]{0,1:T(8,128)(2,1)} copy(bf16[16384,128]{1,0:T(8,128)(2,1)} %get-tuple-element.414) | data formatting | bytes 8388608
  94.7 1.0 broadcast_in_dim.22
  95.7 16.0 %while.18 = (s32[]{:T(128)}, f32[1,2,1024]{2,1,0:T(2,128)S(1)}, f32[1,2,1024]{2,1,0:T(2,128)S(1)}, f32[1,2,1024,128]{3,2,1,0:T(8,128)}, s32[]{:T(128)}, /*index=...) while((s32[]{:T(128)}, f32[1,2,1024]{2,1,0:T(2,128)S(1)}, ...), condition=%wide.region_5.6_spmd.clone, body=%wide.region_0.5_spmd.clone.sunk | while | flops 415243776 | bytes 17719616 | solution.py:93
  95.7 7.0 %conditional.3 = ((f32[1,2,1024]{2,1,0:T(2,128)S(1)}, f32[1,2,1024]{2,1,0:T(2,128)S(1)}, f32[1,2,1024,128]{3,2,1,0:T(8,128)})) conditional(s32[]{:T(128)} %convert_element_type.84, (f32[1,2,1024]{2,1,0:T(2,128)S(1)}, f32[1,2,1024]{2,1,0:T(2,128)S(1)}, f32[1,2,1024,128]{3,2,1,0:T(8,128)}) %tuple.65, (s32[]{:T(128)}, s32[512]{0:T(512)S(1)}, s32[]{:T(128)}, ...), branch_computations={%region_1.0_spmd, %region_2.4_spmd} | conditional | flops 415243776 | bytes 17713234 | solution.py:91
  98.1 3.6 fusion.11
  102.8 7.0 %conditional.3 = ((f32[1,2,1024]{2,1,0:T(2,128)S(1)}, f32[1,2,1024]{2,1,0:T(2,128)S(1)}, f32[1,2,1024,128]{3,2,1,0:T(8,128)})) conditional(s32[]{:T(128)} %convert_element_type.84, (f32[1,2,1024]{2,1,0:T(2,128)S(1)}, f32[1,2,1024]{2,1,0:T(2,128)S(1)}, f32[1,2,1024,128]{3,2,1,0:T(8,128)}) %tuple.65, (s32[]{:T(128)}, s32[512]{0:T(512)S(1)}, s32[]{:T(128)}, ...), branch_computations={%region_1.0_spmd, %region_2.4_spmd} | conditional | flops 415243776 | bytes 17713234 | solution.py:91
  104.1 1.0 fusion.4
  105.2 3.6 fusion.11
  111.8 1.6 broadcast_divide_fusion
  114.6 5.3 all-to-all-start
  119.9 5.3 all-to-all-done
  125.4 3.1 multiply_reduce_fusion
  129.5 1.6 convolution_convert_fusion.1
  131.2 3.2 reshape.225
  134.4 235.9 %all_to_all.26 = bf16[16,20,2048]{2,1,0:T(8,128)(2,1)S(1)} all-to-all(bf16[16,20,2048]{2,1,0:T(8,128)(2,1)} %reshape.225), channel_id=1, replica_groups=mesh['sp'=16,'tp'=8] {'sp'}, dimensions={0} | all-to-all | bytes 2621440 | tf_op jit(solution)/shard_map/all_to_all | solution.py:140
  370.3 1.8 copy.95
  372.4 56.1 %all-gather.6.cloned.1.call-done = bf16[16,160,2048]{2,0,1:T(8,128)(2,1)} async-done(((bf16[16,20,2048]{2,0,1:T(8,128)(2,1)}), bf16[16,160,2048]{2,0,1:T(8,128)(2,1)}) %all-gather.6.cloned.1.call-update) | async-done | bytes 10485776 | tf_op jit(solution)/shard_map/all_gather | solution.py:142
  428.5 13.6 %copy.96 = bf16[16,160,2048]{2,1,0:T(8,128)(2,1)} copy(bf16[16,160,2048]{2,0,1:T(8,128)(2,1)} %all-gather.6.cloned.1.call-done) | data formatting | bytes 20971520 | tf_op jit(solution)/shard_map/all_gather | solution.py:142
  442.1 12.4 %fusion.24 = f32[2560,640]{1,0:T(8,128)S(1)} fusion(bf16[2560,2048]{1,0:T(8,128)(2,1)} %bitcast.85, bf16[1,2048,640]{2,1,0:T(8,128)(2,1)} %param.27), kind=kOutput, calls=%fused_computation.30 | convolution fusion | flops 6710886400 | bytes 19660800 | tf_op jit(solution)/shard_map/dot_general | solution.py:21
  454.5 10.4 %multiply_convert_fusion = bf16[2560,640]{1,0:T(8,128)(2,1)} fusion(f32[2560,640]{1,0:T(8,128)S(1)} %fusion.24, bf16[2560,2048]{1,0:T(8,128)(2,1)S(1)} %bitcast.86, bf16[1,2048,640]{2,1,0:T(8,128)(2,1)S(1)} %copy-done.7), kind=kOutput, calls=%fused_computation.26 | convolution fusion | flops 6720716800 | bytes 22937600 | tf_op jit(solution)/shard_map/dot_general | solution.py:22
  465.0 6.1 dot_general.36
  471.0 12.7 %convolution_convert_fusion = bf16[16,8,20,2048]{3,2,1,0:T(8,128)(2,1)S(1)} fusion(bf16[16,8,20,640]{3,2,1,0:T(8,128)(2,1)} %dot_general.36, bf16[1,640,2048]{2,1,0:T(8,128)(2,1)S(1)} %copy-done), kind=kOutput, calls=%fused_computation.25 | convolution fusion | flops 6716129280 | bytes 16384000 | tf_op jit(solution)/shard_map/dot_general | solution.py:24
  483.8 13.9 %copy.97 = bf16[16,8,20,2048]{3,0,2,1:T(8,128)(2,1)} copy(bf16[16,8,20,2048]{3,2,1,0:T(8,128)(2,1)S(1)} %convolution_convert_fusion) | data formatting | bytes 20971520 | tf_op jit(solution)/shard_map/convert_element_type | solution.py:145
  497.7 62.3 %reduce-scatter.2.cloned.1.call-done = bf16[16,1,20,2048]{3,0,2,1:T(8,128)(2,1)} async-done(((bf16[16,8,20,2048]{3,0,2,1:T(8,128)(2,1)}), bf16[16,1,20,2048]{3,0,2,1:T(8,128)(2,1)}) %reduce-scatter.2.cloned.1.call-update) | async-done | bytes 1310736 | tf_op jit(solution)/shard_map/reduce_scatter | solution.py:144
  560.0 2.0 copy.98
  562.0 30.9 %all_to_all.27 = bf16[16,1,20,2048]{3,2,1,0:T(8,128)(2,1)} all-to-all(bf16[16,1,20,2048]{3,2,1,0:T(8,128)(2,1)S(1)} %copy.98), channel_id=1, replica_groups=mesh['sp'=16,'tp'=8] {'sp'}, dimensions={0} | all-to-all | bytes 2621440 | tf_op jit(solution)/shard_map/all_to_all | solution.py:147
  592.9 3.3 reshape.227
  596.2 2.9 fusion.26
  (153 shorter events, 11.1 us)
Async XLA Ops:
  6.5 464.5 %copy-start = (bf16[1,640,2048]{2,1,0:T(8,128)(2,1)S(1)}, bf16[1,640,2048]{2,1,0:T(8,128)(2,1)}, u32[]{:S(2)}) copy-start(bf16[1,640,2048]{2,1,0:T(8,128)(2,1)} %param.29) | copy-start | bytes 7864324
  6.5 76.0 %all-gather.4.cloned.1.call-start = ((), (), s32[]{:S(2)}) async-start(), calls=%async_computation.4 | async-start | bytes 8912896 | tf_op jit(solution)/shard_map/all_gather | solution.py:12
  95.7 17.9 %copy-start.6 = (f32[128]{0:T(128)S(1)}, f32[128]{0:T(128)}, u32[]{:S(2)}) copy-start(f32[128]{0:T(128)} %param.21) | copy-start | bytes 1540
  111.8 8.0 %copy-start.4 = (s32[128,2]{0,1:T(2,128)S(1)}, s32[128,2]{0,1:T(2,128)}, u32[]{:S(2)}) copy-start(s32[128,2]{0,1:T(2,128)} %param.25) | copy-start | bytes 3076
  111.8 8.1 %copy-start.5 = (f32[128,2]{0,1:T(2,128)S(1)}, f32[128,2]{0,1:T(2,128)}, u32[]{:S(2)}) copy-start(f32[128,2]{0,1:T(2,128)} %param.26) | copy-start | bytes 3076
  113.6 15.9 %copy-start.3 = (f32[2048]{0:T(1024)S(1)}, f32[2048]{0:T(1024)}, u32[]{:S(2)}) copy-start(f32[2048]{0:T(1024)} %param.24) | copy-start | bytes 24580
  114.6 10.7 %all-to-all-start = ((bf16[8,128,128]{2,1,0:T(8,128)(2,1)}), bf16[8,128,128]{2,1,0:T(8,128)(2,1)S(1)}, u32[]{:S(2)}, u32[]{:S(2)}) async-start(bf16[8,128,128]{2,1,0:T(8,128)(2,1)} %multiply_convert_fusion.3), calls=%async_computation | async-start | bytes 524288 | tf_op jit(solution)/shard_map/all_to_all | solution.py:104
  119.8 308.6 %all-gather.6.cloned.1.call-start = ((), (), s32[]{:S(2)}) async-start(), calls=%async_computation.6 | async-start | bytes 11796480 | tf_op jit(solution)/shard_map/all_gather | solution.py:142
  128.5 1.0 copy-start.2
  372.1 187.9 %reduce-scatter.2.cloned.1.call-start = ((), (), s32[]{:S(2)}) async-start(), calls=%async_computation.5 | async-start | bytes 11796480 | tf_op jit(solution)/shard_map/reduce_scatter | solution.py:144
  442.1 12.5 %copy-start.1 = (bf16[16,160,2048]{2,1,0:T(8,128)(2,1)S(1)}, bf16[16,160,2048]{2,1,0:T(8,128)(2,1)}, u32[]{:S(2)}) copy-start(bf16[16,160,2048]{2,1,0:T(8,128)(2,1)} %copy.96) | copy-start | bytes 31457284
  442.1 12.5 %copy-start.7 = (bf16[1,2048,640]{2,1,0:T(8,128)(2,1)S(1)}, bf16[1,2048,640]{2,1,0:T(8,128)(2,1)}, u32[]{:S(2)}) copy-start(bf16[1,2048,640]{2,1,0:T(8,128)(2,1)} %param.28) | copy-start | bytes 7864324
Sparse Core Ops, SparseCore 0:
  9.5 73.0 all-gather.3
  372.2 56.1 all-gather.5
  497.8 62.1 reduce-scatter.1
where the time goes:
time: 608 us; the launch traced here: 606 us
  blocking collectives  267 us (44%)
  waiting for transfers between devices  194 us (32%)
  local copies, waits for them, and re-layouts  62.8 us (10%)
  matrix products  52.5 us (9%)
  between operations  14 us (2%)
  other arithmetic  8.29 us (1%)
    all_to_all x1, blocking collectives, local(): lax.all_to_all(outgoing, 'sp', split_axis=0, concat_axis=0, tiled=True)  236 us
    all_gather x1, waiting for transfers between devices, side_by_side(): lax.all_gather(both, axis, axis=dim, tiled=True)  70 us
    reduce_scatter x1, waiting for transfers between devices, local(): lax.psum_scatter(partial_value.astype(jnp.bfloat16), 'tp', scatter_dimens...  62.3 us
    all_gather x1, waiting for transfers between devices, local(): lax.all_gather(arrived[:, None], 'tp', axis=1, tiled=True)  56.1 us
    all_to_all x1, blocking collectives, local(): lax.all_to_all(summed, 'sp', split_axis=0, concat_axis=0, tiled=True)  30.9 us
    convert_element_type x1, local copies, waits for them, and re-layouts, local(): partial_value.astype(jnp.bfloat16)  13.9 us
    all_gather x1, local copies, waits for them, and re-layouts, local(): lax.all_gather(arrived[:, None], 'tp', axis=1, tiled=True)  13.6 us
    dot_general x1, matrix products, expert_rows(): result = jnp.dot(act, down_local, preferred_element_type=jnp.float32)  12.7 us
  transfers between devices with their start and end apart: 4, of which 4 were waited for; matrix products, arithmetic and copies ran while one was open for 1% of the time, Pallas kernels for 0%

commit v1 on v0

--- a/solution.py
+++ b/solution.py
@@ -5,6 +5,13 @@
 from jax.sharding import PartitionSpec as P
 
 DH = 64
+
+
+def swapped_in(x, mesh_axis, dim):
+    size = lax.axis_size(mesh_axis)
+    blocks = jnp.stack([x for _ in range(size)])
+    blocks = lax.all_to_all(blocks, mesh_axis, split_axis=0, concat_axis=0)
+    return jnp.concatenate(blocks, axis=dim)
 
 
 def side_by_side(arrays, axis, dim, along):
@@ -139,7 +146,7 @@
     down_local = down_weight[0]
     arrived = lax.all_to_all(outgoing, "sp", split_axis=0, concat_axis=0, tiled=True)
     partial_value = expert_rows(
-        lax.all_gather(arrived[:, None], "tp", axis=1, tiled=True), gate_local, up_local, down_local
+        swapped_in(arrived[:, None], "tp", 1), gate_local, up_local, down_local
     )
     summed = lax.psum_scatter(
         partial_value.astype(jnp.bfloat16), "tp", scatter_dimension=1, tiled=True

time: 608 us -> 695 us (1.14)
  blocking collectives: 267 us -> 390 us
  waiting for transfers between devices: 194 us -> 133 us
  local copies, waits for them, and re-layouts: 62.8 us -> 86.5 us
    all_to_all x0 -> x1, blocking collectives: none -> 123 us  [swapped_in(): blocks = lax.all_to_all(blocks, mesh_axis, split_axis=0, concat_axis=0)]
    all_gather x1 -> x0, waiting for transfers between devices: 56.1 us -> none  [local(): lax.all_gather(arrived[:, None], 'tp', axis=1, tiled=True)]
    another operation x1 -> x3, local copies, waits for them, and re-layouts: 0.01 us -> 21.8 us  [the longest x1 16.5 us: expert_rows(): flat = rows_in.reshape(-1, rows_in.shape[-1])]
    reshape x0 -> x1, local copies, waits for them, and re-layouts: none -> 16.8 us  [swapped_in(): return jnp.concatenate(blocks, axis=dim)]
    all_gather x1 -> x0, local copies, waits for them, and re-layouts: 13.6 us -> none  [local(): lax.all_gather(arrived[:, None], 'tp', axis=1, tiled=True)]
  transfers between devices with their start and end apart: 4 -> 3, of which waited for: 4 -> 3; matrix products, arithmetic and copies ran while one was open for 1% -> 0% of each run, Pallas kernels for 0% -> 0%
where the time goes in v1:
time: 695 us; the launch traced here: 692 us
  blocking collectives  390 us (56%)
  waiting for transfers between devices  133 us (19%)
  local copies, waits for them, and re-layouts  86.5 us (12%)
  matrix products  52.5 us (8%)
  between operations  14.3 us (2%)
  other arithmetic  8.29 us (1%)
    all_to_all x1, blocking collectives, local(): lax.all_to_all(outgoing, 'sp', split_axis=0, concat_axis=0, tiled=True)  236 us
    all_to_all x1, blocking collectives, swapped_in(): blocks = lax.all_to_all(blocks, mesh_axis, split_axis=0, concat_axis=0)  123 us
    all_gather x1, waiting for transfers between devices, side_by_side(): lax.all_gather(both, axis, axis=dim, tiled=True)  70 us
    reduce_scatter x1, waiting for transfers between devices, local(): lax.psum_scatter(partial_value.astype(jnp.bfloat16), 'tp', scatter_dimens...  58.1 us
    all_to_all x1, blocking collectives, local(): lax.all_to_all(summed, 'sp', split_axis=0, concat_axis=0, tiled=True)  30.9 us
    reshape x1, local copies, waits for them, and re-layouts, swapped_in(): return jnp.concatenate(blocks, axis=dim)  16.8 us
    another operation x1, local copies, waits for them, and re-layouts, expert_rows(): flat = rows_in.reshape(-1, rows_in.shape[-1])  16.5 us
  transfers between devices with their start and end apart: 3, of which 3 were waited for; matrix products, arithmetic and copies ran while one was open for 0% of the time, Pallas kernels for 0%

profile of v1, /device:TPU:9, one launch (start us, length us, event | category | flops | bytes accessed | tf_op | source)
XLA Modules:
  0.0 692.5 jit_solution(8394809377020082909)
XLA Ops:
  6.5 2.0 pad_maximum_fusion
  11.5 1.1 copy.76
  12.6 70.0 %all-gather.2.cloned.1.call-done = bf16[16384,256]{1,0:T(8,128)(2,1)} async-done(((bf16[1024,256]{1,0:T(8,128)(2,1)}), bf16[16384,256]{1,0:T(8,128)(2,1)}) %all-gather.2.cloned.1.call-update) | async-done | bytes 8388624 | tf_op jit(solution)/shard_map/all_gather | solution.py:19
  82.6 5.7 fusion.36
  88.3 6.4 copy.77
  94.7 1.0 broadcast_in_dim.20
  95.7 16.0 %while.18 = (s32[]{:T(128)}, f32[1,2,1024]{2,1,0:T(2,128)S(1)}, f32[1,2,1024]{2,1,0:T(2,128)S(1)}, f32[1,2,1024,128]{3,2,1,0:T(8,128)}, s32[]{:T(128)}, /*index=...) while((s32[]{:T(128)}, f32[1,2,1024]{2,1,0:T(2,128)S(1)}, ...), condition=%wide.region_5.6_spmd.clone, body=%wide.region_0.5_spmd.clone.sunk | while | flops 415243776 | bytes 17719616 | solution.py:100
  95.7 7.0 %conditional.3 = ((f32[1,2,1024]{2,1,0:T(2,128)S(1)}, f32[1,2,1024]{2,1,0:T(2,128)S(1)}, f32[1,2,1024,128]{3,2,1,0:T(8,128)})) conditional(s32[]{:T(128)} %convert_element_type.84, (f32[1,2,1024]{2,1,0:T(2,128)S(1)}, f32[1,2,1024]{2,1,0:T(2,128)S(1)}, f32[1,2,1024,128]{3,2,1,0:T(8,128)}) %tuple.64, (s32[]{:T(128)}, s32[512]{0:T(512)S(1)}, s32[]{:T(128)}, ...), branch_computations={%region_1.0_spmd, %region_2.4_spmd} | conditional | flops 415243776 | bytes 17713234 | solution.py:98
  98.1 3.6 fusion.11
  102.8 7.0 %conditional.3 = ((f32[1,2,1024]{2,1,0:T(2,128)S(1)}, f32[1,2,1024]{2,1,0:T(2,128)S(1)}, f32[1,2,1024,128]{3,2,1,0:T(8,128)})) conditional(s32[]{:T(128)} %convert_element_type.84, (f32[1,2,1024]{2,1,0:T(2,128)S(1)}, f32[1,2,1024]{2,1,0:T(2,128)S(1)}, f32[1,2,1024,128]{3,2,1,0:T(8,128)}) %tuple.64, (s32[]{:T(128)}, s32[512]{0:T(512)S(1)}, s32[]{:T(128)}, ...), branch_computations={%region_1.0_spmd, %region_2.4_spmd} | conditional | flops 415243776 | bytes 17713234 | solution.py:98
  105.2 3.6 fusion.11
  111.8 1.6 broadcast_divide_fusion
  114.6 5.3 all-to-all-start
  119.9 5.3 all-to-all-done
  125.4 3.1 multiply_reduce_fusion
  129.6 1.6 convolution_convert_fusion.1
  131.2 3.2 reshape.227
  134.4 235.9 %all_to_all.31 = bf16[16,20,2048]{2,1,0:T(8,128)(2,1)S(1)} all-to-all(bf16[16,20,2048]{2,1,0:T(8,128)(2,1)} %reshape.227), channel_id=1, replica_groups=mesh['sp'=16,'tp'=8] {'sp'}, dimensions={0} | all-to-all | bytes 2621440 | tf_op jit(solution)/shard_map/all_to_all | solution.py:147
  371.0 5.4 stack.3
  376.4 123.5 %all_to_all.32 = bf16[8,16,1,20,2048]{4,1,3,2,0:T(8,128)(2,1)S(1)} all-to-all(bf16[8,16,1,20,2048]{4,1,3,2,0:T(8,128)(2,1)} %stack.3), channel_id=1, replica_groups=mesh['sp'=16,'tp'=8] {'tp'}, dimensions={0} | all-to-all | bytes 20971520 | tf_op jit(solution)/shard_map/all_to_all | solution.py:13
  499.9 16.8 %copy.84 = bf16[16,8,1,20,2048]{4,3,1,0,2:T(8,128)(2,1)} copy(bf16[16,8,1,20,2048]{4,0,3,2,1:T(8,128)(2,1)S(1)} %bitcast.87) | data formatting | bytes 20971520 | tf_op jit(solution)/shard_map/reshape | solution.py:14
  516.7 16.5 %reshape_reshape.3 = bf16[2560,2048]{1,0:T(8,128)(2,1)} reshape(bf16[16,8,1,20,2048]{4,3,1,0,2:T(8,128)(2,1)} %copy.84) | data formatting | bytes 20971520 | tf_op jit(solution)/shard_map/reshape;reshape | solution.py:27
  533.2 12.4 %fusion.24 = f32[2560,640]{1,0:T(8,128)S(1)} fusion(bf16[2560,2048]{1,0:T(8,128)(2,1)} %reshape_reshape.3, bf16[1,2048,640]{2,1,0:T(8,128)(2,1)} %param.27), kind=kOutput, calls=%fused_computation.30 | convolution fusion | flops 6710886400 | bytes 19660800 | tf_op jit(solution)/shard_map/dot_general | solution.py:28
  545.6 10.4 %multiply_convert_fusion = bf16[2560,640]{1,0:T(8,128)(2,1)} fusion(f32[2560,640]{1,0:T(8,128)S(1)} %fusion.24, bf16[2560,2048]{1,0:T(8,128)(2,1)S(1)} %copy-done.1, bf16[1,2048,640]{2,1,0:T(8,128)(2,1)S(1)} %copy-done.7), kind=kOutput, calls=%fused_computation.26 | convolution fusion | flops 6720716800 | bytes 22937600 | tf_op jit(solution)/shard_map/dot_general | solution.py:29
  556.0 6.1 dot_general.36
  562.1 12.7 %convolution_convert_fusion = bf16[16,8,20,2048]{3,2,1,0:T(8,128)(2,1)S(1)} fusion(bf16[16,8,20,640]{3,2,1,0:T(8,128)(2,1)} %dot_general.36, bf16[1,640,2048]{2,1,0:T(8,128)(2,1)S(1)} %copy-done), kind=kOutput, calls=%fused_computation.25 | convolution fusion | flops 6716129280 | bytes 16384000 | tf_op jit(solution)/shard_map/dot_general | solution.py:31
  574.8 13.6 %copy.85 = bf16[16,8,20,2048]{3,0,2,1:T(8,128)(2,1)} copy(bf16[16,8,20,2048]{3,2,1,0:T(8,128)(2,1)S(1)} %convolution_convert_fusion) | data formatting | bytes 20971520 | tf_op jit(solution)/shard_map/convert_element_type | solution.py:152
  588.5 58.1 %reduce-scatter.2.cloned.1.call-done = bf16[16,1,20,2048]{3,0,2,1:T(8,128)(2,1)} async-done(((bf16[16,8,20,2048]{3,0,2,1:T(8,128)(2,1)}), bf16[16,1,20,2048]{3,0,2,1:T(8,128)(2,1)}) %reduce-scatter.2.cloned.1.call-update) | async-done | bytes 1310736 | tf_op jit(solution)/shard_map/reduce_scatter | solution.py:151
  646.5 2.0 copy.86
  648.6 30.9 %all_to_all.33 = bf16[16,1,20,2048]{3,2,1,0:T(8,128)(2,1)} all-to-all(bf16[16,1,20,2048]{3,2,1,0:T(8,128)(2,1)S(1)} %copy.86), channel_id=1, replica_groups=mesh['sp'=16,'tp'=8] {'sp'}, dimensions={0} | all-to-all | bytes 2621440 | tf_op jit(solution)/shard_map/all_to_all | solution.py:154
  679.5 3.3 reshape.229
  682.7 2.9 fusion.26
  (153 shorter events, 12.6 us)
Async XLA Ops:
  6.5 555.6 %copy-start = (bf16[1,640,2048]{2,1,0:T(8,128)(2,1)S(1)}, bf16[1,640,2048]{2,1,0:T(8,128)(2,1)}, u32[]{:S(2)}) copy-start(bf16[1,640,2048]{2,1,0:T(8,128)(2,1)} %param.29) | copy-start | bytes 7864324
  6.5 76.0 %all-gather.2.cloned.1.call-start = ((), (), s32[]{:S(2)}) async-start(), calls=%async_computation.5 | async-start | bytes 8912896 | tf_op jit(solution)/shard_map/all_gather | solution.py:19
  95.7 17.9 %copy-start.6 = (f32[128]{0:T(128)S(1)}, f32[128]{0:T(128)}, u32[]{:S(2)}) copy-start(f32[128]{0:T(128)} %param.21) | copy-start | bytes 1540
  111.8 8.0 %copy-start.4 = (s32[128,2]{0,1:T(2,128)S(1)}, s32[128,2]{0,1:T(2,128)}, u32[]{:S(2)}) copy-start(s32[128,2]{0,1:T(2,128)} %param.25) | copy-start | bytes 3076
  111.8 8.1 %copy-start.5 = (f32[128,2]{0,1:T(2,128)S(1)}, f32[128,2]{0,1:T(2,128)}, u32[]{:S(2)}) copy-start(f32[128,2]{0,1:T(2,128)} %param.26) | copy-start | bytes 3076
  113.6 15.9 %copy-start.3 = (f32[2048]{0:T(1024)S(1)}, f32[2048]{0:T(1024)}, u32[]{:S(2)}) copy-start(f32[2048]{0:T(1024)} %param.24) | copy-start | bytes 24580
  114.6 10.7 %all-to-all-start = ((bf16[8,128,128]{2,1,0:T(8,128)(2,1)}), bf16[8,128,128]{2,1,0:T(8,128)(2,1)S(1)}, u32[]{:S(2)}, u32[]{:S(2)}) async-start(bf16[8,128,128]{2,1,0:T(8,128)(2,1)} %multiply_convert_fusion.3), calls=%async_computation | async-start | bytes 524288 | tf_op jit(solution)/shard_map/all_to_all | solution.py:111
  119.8 526.7 %reduce-scatter.2.cloned.1.call-start = ((), (), s32[]{:S(2)}) async-start(), calls=%async_computation.6 | async-start | bytes 11796480 | tf_op jit(solution)/shard_map/reduce_scatter | solution.py:151
  128.5 1.0 copy-start.2
  533.2 12.4 %copy-start.1 = (bf16[2560,2048]{1,0:T(8,128)(2,1)S(1)}, bf16[2560,2048]{1,0:T(8,128)(2,1)}, u32[]{:S(2)}) copy-start(bf16[2560,2048]{1,0:T(8,128)(2,1)} %reshape_reshape.3) | copy-start | bytes 31457284
  533.2 12.4 %copy-start.7 = (bf16[1,2048,640]{2,1,0:T(8,128)(2,1)S(1)}, bf16[1,2048,640]{2,1,0:T(8,128)(2,1)}, u32[]{:S(2)}) copy-start(bf16[1,2048,640]{2,1,0:T(8,128)(2,1)} %param.28) | copy-start | bytes 7864324
Sparse Core Ops, SparseCore 0:
  9.5 73.0 all-gather.1
  588.6 57.8 reduce-scatter.1
